TPU v7x, 32 devices: a whole 2x2x4 slice. The times are simulated.
32 devices in a mesh: sp: 8 (over z, y), tp: 4 (over x, core).
Axes of the slice: x: 2, y: 2, z: 4, core: 2. Of those that a mesh axis runs over, the one named last changes fastest.
Arguments:
- tokens: bfloat16 [3072, 2048], P('sp', 'tp'), may hold values from -6 to 6
- norm_gain: float32 [2048], replicated, may hold values from 0.1 to 1.9
- w_query_down: bfloat16 [2048, 512], replicated, may hold values from -0.125 to 0.125
- query_gain: float32 [512], replicated, may hold values from 0.1 to 1.9
- w_query_up: bfloat16 [512, 1536], P(None, 'tp'), may hold values from -0.25 to 0.25
- w_latent_down: bfloat16 [2048, 256], replicated, may hold values from -0.125 to 0.125
- latent_gain: float32 [256], replicated, may hold values from 0.1 to 1.9
- w_rotary_key: bfloat16 [2048, 32], replicated, may hold values from -0.125 to 0.125
- w_latent_up: bfloat16 [256, 2048], P(None, 'tp'), may hold values from -0.375 to 0.375
- query_head_gain: float32 [96], replicated, may hold values from 0.1 to 1.9
- key_head_gain: float32 [96], replicated, may hold values from 0.1 to 1.9
- w_pool_in: bfloat16 [2048, 1024], P(None, 'tp'), may hold values from -0.125 to 0.125
- w_pool_mix: bfloat16 [4, 256, 256], P('tp'), may hold values from -0.375 to 0.375
- pool_scale: float32 [1024], P('tp'), may hold values from 0.1 to 1.9
- w_attn_out: bfloat16 [1024, 2048], P('tp'), may hold values from -12 to 12
- w_pool_out: bfloat16 [1024, 2048], P('tp'), may hold values from -0.5 to 0.5
- w_gate_attn: bfloat16 [2048, 2048], P(None, 'tp'), may hold values from -0.125 to 0.125
- w_gate_pool: bfloat16 [2048, 2048], P(None, 'tp'), may hold values from -0.125 to 0.125
Outputs:
- mixed: bfloat16 [3072, 2048], P('sp', 'tp')
All inputs are finite; a program needn't handle non-finite values.
Results may differ from a plain program's by a relative error of at most 0.02.
Values may be sent and summed in bfloat16 or wider, within the bound.
A program may use at most 128 MiB of HBM per device.

v0:
```python
import jax
import jax.numpy as jnp
from jax import lax
from jax.sharding import PartitionSpec as P

NOPE = 64
ROPE = 32
VALUE_DIM = 64
POOL_GROUPS = 4
POOL_GROUP = 256


eps = 1e-06
theta = 10000.0


def extended(cells, sides, width):
    for axis, dim in sides:
        count = lax.axis_size(axis)
        ends = count - 1
        head = lax.slice_in_dim(cells, 0, width, axis=dim)
        tail = lax.slice_in_dim(cells, cells.shape[dim] - width, cells.shape[dim], axis=dim)
        cells = jnp.concatenate(
            [
                lax.ppermute(tail, axis, [(i, (i + 1) % count) for i in range(ends)]),
                cells,
                lax.ppermute(head, axis, [((i + 1) % count, i) for i in range(ends)]),
            ],
            axis=dim,
        )
    return cells


def rms_scale(values, gain):
    values = values.astype(jnp.float32)
    return values * lax.rsqrt(jnp.mean(values * values, axis=-1, keepdims=True) + eps) * gain


def rotate(values, positions):
    half = values.shape[-1] // 2
    freqs = theta ** (-jnp.arange(half, dtype=jnp.float32) / half)
    angles = positions.astype(jnp.float32)[:, None] * freqs[None, :]
    cosine = jnp.cos(angles)[:, None, :]
    sine = jnp.sin(angles)[:, None, :]
    first = values[..., :half]
    second = values[..., half:]
    return jnp.concatenate(
        [first * cosine - second * sine, first * sine + second * cosine], axis=-1
    )


def head_finish(values, gain, positions):
    normed = rms_scale(values, gain)
    return jnp.concatenate([normed[..., :NOPE], rotate(normed[..., NOPE:], positions)], axis=-1)


def body(
    tokens,
    norm_gain,
    w_query_down,
    query_gain,
    w_query_up,
    w_latent_down,
    latent_gain,
    w_rotary_key,
    w_latent_up,
    query_head_gain,
    key_head_gain,
    w_pool_in,
    w_pool_mix,
    pool_scale,
    w_attn_out,
    w_pool_out,
    w_gate_attn,
    w_gate_pool,
):
    bf = jnp.bfloat16
    rows = tokens.shape[0]
    length = rows * lax.axis_size("sp")
    local_heads = w_query_up.shape[1] // (NOPE + ROPE)
    positions = lax.axis_index("sp") * rows + jnp.arange(rows, dtype=jnp.int32)
    whole = lax.all_gather(tokens, "tp", axis=1, tiled=True)
    normed = rms_scale(whole, norm_gain).astype(bf)
    query_latent = jnp.dot(normed, w_query_down, preferred_element_type=jnp.float32).astype(bf)
    query_normed = rms_scale(query_latent, query_gain).astype(bf)
    query_raw = jnp.dot(query_normed, w_query_up, preferred_element_type=jnp.float32).astype(bf)
    query_raw = query_raw.reshape(rows, local_heads, NOPE + ROPE)
    query = (head_finish(query_raw, query_head_gain, positions) * (NOPE + ROPE) ** (-0.5)).astype(
        bf
    )
    latent = jnp.dot(normed, w_latent_down, preferred_element_type=jnp.float32).astype(bf)
    key_latent = rms_scale(latent, latent_gain).astype(bf)
    rotary_key = jnp.dot(normed, w_rotary_key, preferred_element_type=jnp.float32).astype(bf)
    start_state = (
        jnp.full((local_heads, rows), -1e30, jnp.float32),
        jnp.zeros((local_heads, rows), jnp.float32),
        jnp.zeros((local_heads, rows, VALUE_DIM), jnp.float32),
    )
    latent_piece = lax.all_gather(key_latent, "sp", axis=0, tiled=True)
    rotary_piece = lax.all_gather(rotary_key, "sp", axis=0, tiled=True)
    blocks = latent_piece.shape[0] // rows
    latent_blocks = latent_piece.reshape(blocks, rows, latent_piece.shape[1])
    rotary_blocks = rotary_piece.reshape(blocks, rows, rotary_piece.shape[1])

    def one_block(state, items):
        latent_block, rotary_block, number = items
        top, total, summed = state
        key_positions = number * rows + jnp.arange(rows, dtype=jnp.int32)
        keys_values = jnp.dot(latent_block, w_latent_up, preferred_element_type=jnp.float32).astype(
            bf
        )
        keys_values = keys_values.reshape(rows, local_heads, NOPE + VALUE_DIM)
        key_raw = jnp.concatenate(
            [
                keys_values[..., :NOPE],
                jnp.broadcast_to(rotary_block[:, None, :], (rows, local_heads, ROPE)),
            ],
            axis=-1,
        )
        key = head_finish(key_raw, key_head_gain, key_positions).astype(bf)
        values = keys_values[..., NOPE:]
        scores = jnp.einsum("qhd,khd->hqk", query, key, preferred_element_type=jnp.float32)
        new_top = jnp.maximum(top, jnp.max(scores, axis=-1))
        factor = jnp.exp(top - new_top)
        expo = jnp.exp(scores - new_top[..., None])
        total = total * factor + jnp.sum(expo, axis=-1)
        summed = summed * factor[..., None] + jnp.einsum(
            "hqk,khv->hqv", expo.astype(bf), values, preferred_element_type=jnp.float32
        )
        return ((new_top, total, summed), None)

    state, _ = lax.scan(
        one_block, start_state, (latent_blocks, rotary_blocks, jnp.arange(blocks, dtype=jnp.int32))
    )
    top, total, summed = state
    attn_rows = jnp.transpose(summed / total[..., None], (1, 0, 2)).reshape(
        rows, local_heads * VALUE_DIM
    )
    attn_rows = attn_rows.astype(bf)
    pool_input = jnp.dot(normed, w_pool_in, preferred_element_type=jnp.float32).astype(bf)
    reach = 2**POOL_GROUPS // 2
    padded = extended(pool_input, (("sp", 0),), reach).astype(jnp.float32)
    local_groups = w_pool_mix.shape[0]
    group_ids = lax.axis_index("tp") * local_groups + jnp.arange(local_groups, dtype=jnp.int32)
    windows = jnp.power(2, group_ids + 1)
    channel_window = jnp.repeat(windows, POOL_GROUP)
    pooled = jnp.zeros((rows, local_groups * POOL_GROUP), jnp.float32)
    for shift in range(-reach, reach):
        inside = (shift >= -(channel_window // 2)) & (
            shift <= channel_window - channel_window // 2 - 1
        )
        pooled = pooled + jnp.where(
            inside[None, :], padded[reach + shift : reach + shift + rows], 0.0
        )
    low = jnp.clip(positions[:, None] - channel_window[None, :] // 2, 0, length)
    high = jnp.clip(
        positions[:, None] + channel_window[None, :] - channel_window[None, :] // 2, 0, length
    )
    count = (high - low).astype(jnp.float32)
    pool_mixed = (pooled / count - pool_input.astype(jnp.float32)).astype(bf)
    pool_mixed = pool_mixed.reshape(rows, local_groups, POOL_GROUP)
    grouped = jnp.einsum("lgc,gcd->lgd", pool_mixed, w_pool_mix, preferred_element_type=jnp.float32)
    pool_rows = (grouped.reshape(rows, local_groups * POOL_GROUP) * pool_scale).astype(bf)
    gate_attn = jax.nn.sigmoid(jnp.dot(normed, w_gate_attn, preferred_element_type=jnp.float32))
    gate_pool = jax.nn.sigmoid(jnp.dot(normed, w_gate_pool, preferred_element_type=jnp.float32))
    attn_tokens, pool_tokens = (
        lax.all_to_all(attn_rows, "tp", split_axis=0, concat_axis=1, tiled=True),
        lax.all_to_all(pool_rows, "tp", split_axis=0, concat_axis=1, tiled=True),
    )
    attn_weight, pool_weight = (
        lax.all_gather(w_attn_out, "tp", axis=0, tiled=True),
        lax.all_gather(w_pool_out, "tp", axis=0, tiled=True),
    )
    attn_here = jnp.dot(attn_tokens, attn_weight, preferred_element_type=jnp.float32)
    pool_here = jnp.dot(pool_tokens, pool_weight, preferred_element_type=jnp.float32)
    attn_branch, pool_branch = (
        lax.all_to_all(
            attn_here.astype(jnp.bfloat16), "tp", split_axis=1, concat_axis=0, tiled=True
        ).astype(attn_here.dtype),
        lax.all_to_all(
            pool_here.astype(jnp.bfloat16), "tp", split_axis=1, concat_axis=0, tiled=True
        ).astype(pool_here.dtype),
    )
    return (gate_attn * attn_branch + gate_pool * pool_branch).astype(bf)


def solution(mesh):
    placed = (
        P("sp", "tp"),
        P(),
        P(),
        P(),
        P(None, "tp"),
        P(),
        P(),
        P(),
        P(None, "tp"),
        P(),
        P(),
        P(None, "tp"),
        P("tp", None, None),
        P("tp"),
        P("tp", None),
        P("tp", None),
        P(None, "tp"),
        P(None, "tp"),
    )
    return jax.shard_map(body, mesh=mesh, in_specs=placed, out_specs=P("sp", "tp"), check_vma=False)
```

profile of v0, /device:TPU:1, one launch (start us, length us, event | category | flops | bytes accessed | tf_op | source)
XLA Modules:
  0.0 211.8 jit_solution(344831506499883668)
XLA Ops:
  7.3 23.7 %all-gather.5.cloned.1.call-done = bf16[384,2048]{1,0:T(8,128)(2,1)} async-done(((bf16[384,512]{1,0:T(8,128)(2,1)}), bf16[384,2048]{1,0:T(8,128)(2,1)}) %all-gather.5.cloned.1.call-update) | async-done | bytes 1572880 | tf_op jit(solution)/shard_map/all_gather | solution.py:82
  31.0 1.8 fusion.19
  32.8 2.6 %multiply_reduce_fusion.1 = (f32[384]{0:T(512)S(1)}, f32[384,256]{0,1:T(8,128)S(1)}) fusion(bf16[2048,256]{1,0:T(8,128)(2,1)} %param.25, bf16[384,2048]{1,0:T(8,128)(2,1)} %all-gather.5.cloned.1.call-done, f32[2048]{0:T(1024)} %param.21, f32[384]{0:T(512)S(1)} %add_rsqrt_fusion.4), kind=kOutput, calls=%fused_computation.112 | convolution fusion | flops 406191744 | bytes 3025920 | tf_op jit(solution)/shard_map/dot_general | solution.py:91
  38.1 2.6 %multiply_reduce_fusion = (f32[384]{0:T(512)S(1)}, f32[384,512]{1,0:T(8,128)S(1)}) fusion(bf16[2048,512]{1,0:T(8,128)(2,1)S(1)} %copy-done, bf16[384,2048]{1,0:T(8,128)(2,1)} %all-gather.5.cloned.1.call-done, f32[2048]{0:T(1024)S(1)} %copy-done.15, f32[384]{0:T(512)S(1)} %add_rsqrt_fusion.4), kind=kOutput, calls=%fused_computation.65 | convolution fusion | flops 809238144 | bytes 4467712 | tf_op jit(solution)/shard_map/dot_general | solution.py:84
  43.0 1.3 collective-permute-start.1
  44.3 4.0 %collective-permute-start = (bf16[8,256]{1,0:T(8,128)(2,1)S(1)}, bf16[8,256]{1,0:T(8,128)(2,1)S(1)}, u32[]{:S(2)}, u32[]{:S(2)}) collective-permute-start(bf16[8,256]{1,0:T(8,128)(2,1)S(1)} %get-tuple-element.153), channel_id=1, source_target_pairs={{0,4},{4,8},{8,12},{12,16},{16,20},{20,24},{24,28},{1,5},{5,9},{9,... | collective-permute-start | bytes 12296 | tf_op jit(solution)/shard_map/ppermute | solution.py:25
  49.7 25.2 %all_gather.17 = bf16[3072,32]{0,1:T(8,128)(2,1)S(1)} all-gather(bf16[384,32]{0,1:T(8,128)(2,1)S(1)} %convolution_convert_fusion.7), channel_id=1, replica_groups=mesh['sp'=8,'tp'=4] {'sp'}, dimensions={0}, use_global_device_ids=true | all-gather | bytes 221184 | tf_op jit(solution)/shard_map/all_gather | solution.py:100
  75.6 1.4 fusion.58
  77.8 11.5 %all-to-all-start.2 = ((bf16[4,96,256]{2,1,0:T(8,128)(2,1)}), bf16[4,96,256]{2,1,0:T(8,128)(2,1)}, u32[]{:S(2)}, u32[]{:S(2)}) async-start(bf16[4,96,256]{2,1,0:T(8,128)(2,1)} %multiply_convert_fusion.2), calls=%async_computation.2 | async-start | bytes 393216 | tf_op jit(solution)/shard_map/all_to_all | solution.py:168
  89.3 2.7 %copy.46 = bf16[3072,256]{1,0:T(8,128)(2,1)} copy(bf16[3072,256]{0,1:T(8,128)(2,1)} %all-gather.7.cloned.1.call-done) | data formatting | bytes 3145728
  92.0 73.4 %while.15 = (s32[]{:T(128)}, f32[4,384]{1,0:T(4,128)S(1)}, f32[4,384]{1,0:T(4,128)S(1)}, f32[4,384,64]{1,2,0:T(8,128)S(1)}, bf16[8,384,256]{2,1,0:T(8,128)(2,1)}...) while((s32[]{:T(128)}, f32[4,384]{1,0:T(4,128)S(1)}, ...), condition=%wide.region_8.9_spmd.clone, body=%wide.region_4.8_spmd.clone.sunk | while | flops 295714592 | bytes 23564012 | solution.py:132
  92.7 1.3 convolution_convert_fusion.9
  96.1 2.0 bitcast_reduce_fusion.2
  98.1 2.1 %fusion.99 = f32[4,384]{1,0:T(4,128)S(1)} fusion(f32[4,384,384]{2,1,0:T(8,128)} %get-tuple-element.235, f32[4,384]{1,0:T(4,128)S(1)} %select_maximum_fusion.2), kind=kLoop, calls=%fused_computation.4.clone.1 | loop fusion | flops 1178112 | bytes 2371584 | tf_op jit(solution)/shard_map/while/body/eval_jaxpr/reduce_sum | solution.py:126
  101.8 1.3 convolution_convert_fusion.9
  105.2 2.0 bitcast_reduce_fusion.2
  107.2 2.1 %fusion.99 = f32[4,384]{1,0:T(4,128)S(1)} fusion(f32[4,384,384]{2,1,0:T(8,128)} %get-tuple-element.235, f32[4,384]{1,0:T(4,128)S(1)} %select_maximum_fusion.2), kind=kLoop, calls=%fused_computation.4.clone.1 | loop fusion | flops 1178112 | bytes 2371584 | tf_op jit(solution)/shard_map/while/body/eval_jaxpr/reduce_sum | solution.py:126
  110.9 1.3 convolution_convert_fusion.9
  114.3 2.0 bitcast_reduce_fusion.2
  116.3 2.2 %fusion.99 = f32[4,384]{1,0:T(4,128)S(1)} fusion(f32[4,384,384]{2,1,0:T(8,128)} %get-tuple-element.235, f32[4,384]{1,0:T(4,128)S(1)} %select_maximum_fusion.2), kind=kLoop, calls=%fused_computation.4.clone.1 | loop fusion | flops 1178112 | bytes 2371584 | tf_op jit(solution)/shard_map/while/body/eval_jaxpr/reduce_sum | solution.py:126
  120.0 1.3 convolution_convert_fusion.9
  123.4 2.0 bitcast_reduce_fusion.2
  125.4 2.3 %fusion.99 = f32[4,384]{1,0:T(4,128)S(1)} fusion(f32[4,384,384]{2,1,0:T(8,128)} %get-tuple-element.235, f32[4,384]{1,0:T(4,128)S(1)} %select_maximum_fusion.2), kind=kLoop, calls=%fused_computation.4.clone.1 | loop fusion | flops 1178112 | bytes 2371584 | tf_op jit(solution)/shard_map/while/body/eval_jaxpr/reduce_sum | solution.py:126
  129.8 1.3 convolution_convert_fusion.9
  133.2 2.0 bitcast_reduce_fusion.2
  135.2 2.1 %fusion.99 = f32[4,384]{1,0:T(4,128)S(1)} fusion(f32[4,384,384]{2,1,0:T(8,128)} %get-tuple-element.235, f32[4,384]{1,0:T(4,128)S(1)} %select_maximum_fusion.2), kind=kLoop, calls=%fused_computation.4.clone.1 | loop fusion | flops 1178112 | bytes 2371584 | tf_op jit(solution)/shard_map/while/body/eval_jaxpr/reduce_sum | solution.py:126
  138.9 1.3 convolution_convert_fusion.9
  142.3 2.0 bitcast_reduce_fusion.2
  144.3 2.1 %fusion.99 = f32[4,384]{1,0:T(4,128)S(1)} fusion(f32[4,384,384]{2,1,0:T(8,128)} %get-tuple-element.235, f32[4,384]{1,0:T(4,128)S(1)} %select_maximum_fusion.2), kind=kLoop, calls=%fused_computation.4.clone.1 | loop fusion | flops 1178112 | bytes 2371584 | tf_op jit(solution)/shard_map/while/body/eval_jaxpr/reduce_sum | solution.py:126
  148.0 1.4 convolution_convert_fusion.9
  151.4 2.0 bitcast_reduce_fusion.2
  153.4 2.1 %fusion.99 = f32[4,384]{1,0:T(4,128)S(1)} fusion(f32[4,384,384]{2,1,0:T(8,128)} %get-tuple-element.235, f32[4,384]{1,0:T(4,128)S(1)} %select_maximum_fusion.2), kind=kLoop, calls=%fused_computation.4.clone.1 | loop fusion | flops 1178112 | bytes 2371584 | tf_op jit(solution)/shard_map/while/body/eval_jaxpr/reduce_sum | solution.py:126
  157.1 1.3 convolution_convert_fusion.9
  160.5 2.0 bitcast_reduce_fusion.2
  162.5 2.1 %fusion.99 = f32[4,384]{1,0:T(4,128)S(1)} fusion(f32[4,384,384]{2,1,0:T(8,128)} %get-tuple-element.235, f32[4,384]{1,0:T(4,128)S(1)} %select_maximum_fusion.2), kind=kLoop, calls=%fused_computation.4.clone.1 | loop fusion | flops 1178112 | bytes 2371584 | tf_op jit(solution)/shard_map/while/body/eval_jaxpr/reduce_sum | solution.py:126
  165.6 0.8 copy.40
  166.5 3.4 %all-to-all-start = ((bf16[4,96,256]{2,1,0:T(8,128)(2,1)}), bf16[4,96,256]{2,1,0:T(8,128)(2,1)S(1)}, u32[]{:S(2)}, u32[]{:S(2)}) async-start(bf16[4,96,256]{2,1,0:T(8,128)(2,1)} %copy.40), calls=%async_computation | async-start | bytes 393216 | tf_op jit(solution)/shard_map/all_to_all | solution.py:167
  169.9 0.9 copy.52
  170.8 3.1 %all-to-all-done = bf16[4,96,256]{2,1,0:T(8,128)(2,1)S(1)} async-done(((bf16[4,96,256]{2,1,0:T(8,128)(2,1)}), bf16[4,96,256]{2,1,0:T(8,128)(2,1)S(1)}, u32[]{:S(2)}, u32[]{:S(2)}) %all-to-all-start) | async-done | bytes 196640 | tf_op jit(solution)/shard_map/all_to_all | solution.py:167
  174.0 3.0 %convolution_convert_fusion.2 = bf16[96,2048]{1,0:T(8,128)(2,1)S(1)} fusion(bf16[96,1024]{1,0:T(8,128)(2,1)S(1)} %bitcast.121, bf16[1024,2048]{1,0:T(8,128)(2,1)} %all-gather.9.cloned.1.call-done), kind=kOutput, calls=%fused_computation.44 | convolution fusion | flops 402849792 | bytes 4784128 | tf_op jit(solution)/shard_map/dot_general | solution.py:174
  177.8 4.6 %all-to-all-start.1 = ((bf16[96,4,512]{2,0,1:T(8,128)(2,1)}), bf16[96,4,512]{2,0,1:T(8,128)(2,1)S(1)}, u32[]{:S(2)}, u32[]{:S(2)}) async-start(bf16[96,4,512]{2,0,1:T(8,128)(2,1)} %bitcast.93), calls=%async_computation.1 | async-start | bytes 786432 | tf_op jit(solution)/shard_map/all_to_all | solution.py:177
  182.4 3.0 %convolution_convert_fusion.1 = bf16[96,2048]{1,0:T(8,128)(2,1)S(1)} fusion(bf16[96,1024]{1,0:T(8,128)(2,1)S(1)} %bitcast.120, bf16[1024,2048]{1,0:T(8,128)(2,1)} %all-gather.11.cloned.1.call-done), kind=kOutput, calls=%fused_computation.43 | convolution fusion | flops 402849792 | bytes 4784128 | tf_op jit(solution)/shard_map/dot_general | solution.py:175
  186.2 2.6 %all-to-all-done.1 = bf16[96,4,512]{2,0,1:T(8,128)(2,1)S(1)} async-done(((bf16[96,4,512]{2,0,1:T(8,128)(2,1)}), bf16[96,4,512]{2,0,1:T(8,128)(2,1)S(1)}, u32[]{:S(2)}, u32[]{:S(2)}) %all-to-all-start.1) | async-done | bytes 393248 | tf_op jit(solution)/shard_map/all_to_all | solution.py:177
  188.9 4.4 %all-to-all-start.3 = ((bf16[96,4,512]{2,0,1:T(8,128)(2,1)}), bf16[96,4,512]{2,0,1:T(8,128)(2,1)S(1)}, u32[]{:S(2)}, u32[]{:S(2)}) async-start(bf16[96,4,512]{2,0,1:T(8,128)(2,1)} %bitcast.92), calls=%async_computation.3 | async-start | bytes 786432 | tf_op jit(solution)/shard_map/all_to_all | solution.py:180
  193.3 1.0 convert_element_type.155
  194.2 5.5 %all-to-all-done.3 = bf16[96,4,512]{2,0,1:T(8,128)(2,1)S(1)} async-done(((bf16[96,4,512]{2,0,1:T(8,128)(2,1)}), bf16[96,4,512]{2,0,1:T(8,128)(2,1)S(1)}, u32[]{:S(2)}, u32[]{:S(2)}) %all-to-all-start.3) | async-done | bytes 393248 | tf_op jit(solution)/shard_map/all_to_all | solution.py:180
  199.8 3.5 %fusion.26 = f32[384,512]{1,0:T(8,128)S(1)} fusion(f32[384,512]{1,0:T(8,128)} %bitcast.122, bf16[2048,512]{1,0:T(8,128)(2,1)} %param.36, bf16[384,2048]{1,0:T(8,128)(2,1)} %all-gather.5.cloned.1.call-done, f32[2048]{0:T(1024)S(1)} %copy-done.15, f32[384]{0:T(512)S(1)} %add_rsqrt_fusion.4), kind=kOutput, calls=%fused_computation.51 | convolution fusion | flops 809238528 | bytes 5252608 | tf_op jit(solution)/shard_map/dot_general | solution.py:164
  203.4 1.9 fusion.31
  (241 shorter events, 33.4 us)
Async XLA Ops:
  6.5 31.5 %copy-start = (bf16[2048,512]{1,0:T(8,128)(2,1)S(1)}, bf16[2048,512]{1,0:T(8,128)(2,1)}, u32[]{:S(2)}) copy-start(bf16[2048,512]{1,0:T(8,128)(2,1)} %param.22) | copy-start | bytes 6291460
  6.5 24.5 %all-gather.5.cloned.1.call-start = ((), (), s32[]{:S(2)}) async-start(), calls=%async_computation.4 | async-start | bytes 1966080 | tf_op jit(solution)/shard_map/all_gather | solution.py:82
  7.3 82.0 %all-gather.7.cloned.1.call-start = ((), (), s32[]{:S(2)}) async-start(), calls=%async_computation.5 | async-start | bytes 1769472 | tf_op jit(solution)/shard_map/all_gather | solution.py:99
  32.8 2.6 %copy-start.8 = (f32[256]{0:T(256)S(1)}, f32[256]{0:T(256)}, u32[]{:S(2)}) copy-start(f32[256]{0:T(256)} %param.26) | copy-start | bytes 3076
  35.4 2.6 %copy-start.15 = (f32[2048]{0:T(1024)S(1)}, f32[2048]{0:T(1024)}, u32[]{:S(2)}) copy-start(f32[2048]{0:T(1024)} %param.21) | copy-start | bytes 24580
  36.3 137.7 %all-gather.9.cloned.1.call-start = ((), (), s32[]{:S(2)}) async-start(), calls=%async_computation.6 | async-start | bytes 5242880 | tf_op jit(solution)/shard_map/all_gather | solution.py:171
  37.0 145.4 %all-gather.11.cloned.1.call-start = ((), (), s32[]{:S(2)}) async-start(), calls=%async_computation.7 | async-start | bytes 5242880 | tf_op jit(solution)/shard_map/all_gather | solution.py:172
  38.0 2.6 %copy-start.5 = (bf16[512,384]{1,0:T(8,128)(2,1)S(1)}, bf16[512,384]{1,0:T(8,128)(2,1)}, u32[]{:S(2)}) copy-start(bf16[512,384]{1,0:T(8,128)(2,1)} %param.24) | copy-start | bytes 1179652
  38.0 2.6 %copy-start.7 = (f32[512]{0:T(512)S(1)}, f32[512]{0:T(512)}, u32[]{:S(2)}) copy-start(f32[512]{0:T(512)} %param.23) | copy-start | bytes 6148
  38.0 3.2 %copy-start.10 = (f32[96]{0:T(128)S(1)}, f32[96]{0:T(128)}, u32[]{:S(2)}) copy-start(f32[96]{0:T(128)} %param.29) | copy-start | bytes 1156
  40.6 1.4 copy-start.3
  40.6 1.7 copy-start.12
  42.3 6.8 %copy-start.13 = (bf16[2048,32]{0,1:T(8,128)(2,1)S(1)}, bf16[2048,32]{0,1:T(8,128)(2,1)}, u32[]{:S(2)}) copy-start(bf16[2048,32]{0,1:T(8,128)(2,1)} %param.27) | copy-start | bytes 393220
  43.0 32.6 %collective-permute-start.1 = (bf16[8,256]{1,0:T(8,128)(2,1)S(1)}, bf16[8,256]{1,0:T(8,128)(2,1)S(1)}, u32[]{:S(2)}, u32[]{:S(2)}) collective-permute-start(bf16[8,256]{1,0:T(8,128)(2,1)S(1)} %get-tuple-element.154), channel_id=1, source_target_pairs={{4,0},{8,4},{12,8},{16,12},{20,16},{24,20},{28,24},{5,1},{9,5},{13... | collective-permute-start | bytes 12296 | tf_op jit(solution)/shard_map/ppermute | solution.py:27
  44.3 31.3 %collective-permute-start = (bf16[8,256]{1,0:T(8,128)(2,1)S(1)}, bf16[8,256]{1,0:T(8,128)(2,1)S(1)}, u32[]{:S(2)}, u32[]{:S(2)}) collective-permute-start(bf16[8,256]{1,0:T(8,128)(2,1)S(1)} %get-tuple-element.153), channel_id=1, source_target_pairs={{0,4},{4,8},{8,12},{12,16},{16,20},{20,24},{24,28},{1,5},{5,9},{9,... | collective-permute-start | bytes 12296 | tf_op jit(solution)/shard_map/ppermute | solution.py:25
  48.3 27.3 %copy-start.14 = (bf16[1,256,256]{2,1,0:T(8,128)(2,1)S(1)}, bf16[1,256,256]{2,1,0:T(8,128)(2,1)}, u32[]{:S(2)}) copy-start(bf16[1,256,256]{2,1,0:T(8,128)(2,1)} %param.32) | copy-start | bytes 393220
  75.6 1.4 copy-start.9
  77.0 14.9 %copy-start.6 = (f32[96]{0:T(128)S(1)}, f32[96]{0:T(128)}, u32[]{:S(2)}) copy-start(f32[96]{0:T(128)} %param.30) | copy-start | bytes 1156
  77.8 88.7 %all-to-all-start.2 = ((bf16[4,96,256]{2,1,0:T(8,128)(2,1)}), bf16[4,96,256]{2,1,0:T(8,128)(2,1)}, u32[]{:S(2)}, u32[]{:S(2)}) async-start(bf16[4,96,256]{2,1,0:T(8,128)(2,1)} %multiply_convert_fusion.2), calls=%async_computation.2 | async-start | bytes 393216 | tf_op jit(solution)/shard_map/all_to_all | solution.py:168
  94.3 1.8 copy-start.2
  98.1 2.4 %copy-start.1 = (f32[4,384,384]{2,1,0:T(8,128)S(1)}, f32[4,384,384]{2,1,0:T(8,128)}, u32[]{:S(2)}) copy-start(f32[4,384,384]{2,1,0:T(8,128)} %get-tuple-element.235) | copy-start | bytes 7077892 | tf_op jit(solution)/shard_map/while
  103.3 1.8 copy-start.2
  107.2 2.4 %copy-start.1 = (f32[4,384,384]{2,1,0:T(8,128)S(1)}, f32[4,384,384]{2,1,0:T(8,128)}, u32[]{:S(2)}) copy-start(f32[4,384,384]{2,1,0:T(8,128)} %get-tuple-element.235) | copy-start | bytes 7077892 | tf_op jit(solution)/shard_map/while
  112.4 1.8 copy-start.2
  116.3 2.4 %copy-start.1 = (f32[4,384,384]{2,1,0:T(8,128)S(1)}, f32[4,384,384]{2,1,0:T(8,128)}, u32[]{:S(2)}) copy-start(f32[4,384,384]{2,1,0:T(8,128)} %get-tuple-element.235) | copy-start | bytes 7077892 | tf_op jit(solution)/shard_map/while
  121.5 1.8 copy-start.2
  125.4 3.1 %copy-start.1 = (f32[4,384,384]{2,1,0:T(8,128)S(1)}, f32[4,384,384]{2,1,0:T(8,128)}, u32[]{:S(2)}) copy-start(f32[4,384,384]{2,1,0:T(8,128)} %get-tuple-element.235) | copy-start | bytes 7077892 | tf_op jit(solution)/shard_map/while
  131.4 1.8 copy-start.2
  135.2 2.4 %copy-start.1 = (f32[4,384,384]{2,1,0:T(8,128)S(1)}, f32[4,384,384]{2,1,0:T(8,128)}, u32[]{:S(2)}) copy-start(f32[4,384,384]{2,1,0:T(8,128)} %get-tuple-element.235) | copy-start | bytes 7077892 | tf_op jit(solution)/shard_map/while
  140.4 1.8 copy-start.2
  144.3 2.4 %copy-start.1 = (f32[4,384,384]{2,1,0:T(8,128)S(1)}, f32[4,384,384]{2,1,0:T(8,128)}, u32[]{:S(2)}) copy-start(f32[4,384,384]{2,1,0:T(8,128)} %get-tuple-element.235) | copy-start | bytes 7077892 | tf_op jit(solution)/shard_map/while
  149.6 1.8 copy-start.2
  153.4 2.4 %copy-start.1 = (f32[4,384,384]{2,1,0:T(8,128)S(1)}, f32[4,384,384]{2,1,0:T(8,128)}, u32[]{:S(2)}) copy-start(f32[4,384,384]{2,1,0:T(8,128)} %get-tuple-element.235) | copy-start | bytes 7077892 | tf_op jit(solution)/shard_map/while
  158.7 1.8 copy-start.2
  162.5 2.4 %copy-start.1 = (f32[4,384,384]{2,1,0:T(8,128)S(1)}, f32[4,384,384]{2,1,0:T(8,128)}, u32[]{:S(2)}) copy-start(f32[4,384,384]{2,1,0:T(8,128)} %get-tuple-element.235) | copy-start | bytes 7077892 | tf_op jit(solution)/shard_map/while
  166.5 7.5 %all-to-all-start = ((bf16[4,96,256]{2,1,0:T(8,128)(2,1)}), bf16[4,96,256]{2,1,0:T(8,128)(2,1)S(1)}, u32[]{:S(2)}, u32[]{:S(2)}) async-start(bf16[4,96,256]{2,1,0:T(8,128)(2,1)} %copy.40), calls=%async_computation | async-start | bytes 393216 | tf_op jit(solution)/shard_map/all_to_all | solution.py:167
  177.8 11.1 %all-to-all-start.1 = ((bf16[96,4,512]{2,0,1:T(8,128)(2,1)}), bf16[96,4,512]{2,0,1:T(8,128)(2,1)S(1)}, u32[]{:S(2)}, u32[]{:S(2)}) async-start(bf16[96,4,512]{2,0,1:T(8,128)(2,1)} %bitcast.93), calls=%async_computation.1 | async-start | bytes 786432 | tf_op jit(solution)/shard_map/all_to_all | solution.py:177
  188.9 10.8 %all-to-all-start.3 = ((bf16[96,4,512]{2,0,1:T(8,128)(2,1)}), bf16[96,4,512]{2,0,1:T(8,128)(2,1)S(1)}, u32[]{:S(2)}, u32[]{:S(2)}) async-start(bf16[96,4,512]{2,0,1:T(8,128)(2,1)} %bitcast.92), calls=%async_computation.3 | async-start | bytes 786432 | tf_op jit(solution)/shard_map/all_to_all | solution.py:180
  199.8 3.6 %copy-start.4 = (bf16[384,2048]{1,0:T(8,128)(2,1)S(1)}, bf16[384,2048]{1,0:T(8,128)(2,1)}, u32[]{:S(2)}) copy-start(bf16[384,2048]{1,0:T(8,128)(2,1)} %all-gather.5.cloned.1.call-done) | copy-start | bytes 4718596
  199.8 3.6 %copy-start.11 = (bf16[2048,512]{1,0:T(8,128)(2,1)S(1)}, bf16[2048,512]{1,0:T(8,128)(2,1)}, u32[]{:S(2)}) copy-start(bf16[2048,512]{1,0:T(8,128)(2,1)} %param.37) | copy-start | bytes 6291460
Sparse Core Ops, SparseCore 0:
  8.9 22.0 all-gather.4
  36.4 44.1 all-gather.6
  82.2 36.1 all-gather.8
  119.8 32.7 all-gather.10
where the time goes:
time: 214 us; the launch traced here: 212 us
  matrix products  50.5 us (24%)
  waiting for transfers between devices  36.9 us (17%)
  starting transfers between devices  29.3 us (14%)
  other arithmetic  26.5 us (12%)
  blocking collectives  25.2 us (12%)
  local copies, waits for them, and re-layouts  23.5 us (11%)
  between operations  13.7 us (6%)
  loops' own time  6.1 us (3%)
    all_gather x1, blocking collectives, body(): rotary_piece = lax.all_gather(rotary_key, 'sp', axis=0, tiled=True)  25.2 us
    all_gather x1, waiting for transfers between devices, body(): whole = lax.all_gather(tokens, 'tp', axis=1, tiled=True)  23.7 us
    reduce_sum x8, other arithmetic, one_block(): total = total * factor + jnp.sum(expo, axis=-1)  17.4 us
    dot_general x8, matrix products, one_block(): jnp.einsum('qhd,khd->hqk', query, key, preferred_element_type=jnp.float32)  16 us
    all_to_all x1, starting transfers between devices, body(): lax.all_to_all(pool_rows, 'tp', split_axis=0, concat_axis=1, tiled=True)  11.5 us
    dot_general x8, matrix products, one_block(): jnp.dot(latent_block, w_latent_up, preferred_element_type=jnp.float32)  10.6 us
    another operation x1, loops' own time, body(): lax.scan(one_block, start_state, (latent_blocks, rotary_blocks, jnp.arang...  6.1 us
    broadcast_in_dim x16, local copies, waits for them, and re-layouts, one_block(): jnp.broadcast_to(rotary_block[:, None, :], (rows, local_heads, ROPE))  6.04 us
  transfers between devices with their start and end apart: 10, of which 4 were waited for; matrix products, arithmetic and copies ran while one was open for 41% of the time, Pallas kernels for 0%

commit v1 on v0

v1 whole, which is shorter than its diff:
```python
import functools
import math

import jax
import jax.numpy as jnp
from jax import lax
from jax.experimental import pallas as pl
from jax.experimental.pallas import tpu as pltpu
from jax.sharding import PartitionSpec as P

NOPE = 64
ROPE = 32
VALUE_DIM = 64
POOL_GROUPS = 4
POOL_GROUP = 256
LANES = 128
REACH = 2**POOL_GROUPS // 2

eps = 1e-06
theta = 10000.0
f32 = jnp.float32
bf = jnp.bfloat16
MESH = pl.DeviceIdType.MESH


def flip(index, offset):
    bit = 1
    while bit <= offset:
        if offset & bit:
            index = index + bit - 2 * bit * ((index // bit) % 2)
        bit *= 2
    return index


def mm(a, b):
    return jnp.dot(a, b, preferred_element_type=f32)


def kernel(
    n,
    m,
    tokens,
    norm_gain,
    query_gain,
    w_query_up,
    latent_gain,
    w_rotary,
    w_latent_up,
    gain_q,
    gain_k,
    w_pool_mix,
    pool_scale,
    cosine,
    sine,
    h_query_down,
    h_latent_down,
    h_pool_in,
    h_gate_attn,
    h_gate_pool,
    h_attn_out,
    h_pool_out,
    out,
    w_query_down,
    w_latent_down,
    w_pool_in,
    w_gate_attn,
    w_gate_pool,
    w_attn_out,
    w_pool_out,
    tok,
    scaled,
    acc_q,
    acc_l,
    acc_r,
    acc_p,
    acc_ga,
    acc_gp,
    queries,
    latents,
    attn_acc,
    padded,
    attn_rows,
    pool_rows,
    local_sem,
    tok_sem,
    wa_sem,
    wp_sem,
    ar_sem,
    pr_sem,
    halo_sem,
    near_sem,
    far_sem,
    main_sem,
    pair_sem,
    pair_send,
):
    s = lax.axis_index("sp")
    t = lax.axis_index("tp")
    rows, cols = tokens.shape
    pairs = n // 2
    p = s // 2
    y = s % 2
    half = rows // 2
    across = flip(s, 1)
    other = (s + n + 2 * y - 1) % n
    heads = attn_acc.shape[0]
    rank = latents.shape[2] - LANES

    def same_parity(i):
        return ((p + i) % pairs) * 2 + y

    fetches = []
    for i, (far, near) in enumerate(
        (
            (h_latent_down, w_latent_down),
            (h_query_down, w_query_down),
            (h_pool_in, w_pool_in),
            (h_gate_attn, w_gate_attn),
            (h_gate_pool, w_gate_pool),
        )
    ):
        fetch = pltpu.make_async_copy(far, near, local_sem.at[i])
        fetch.start()
        fetches.append(fetch)
    mine = pl.ds(pl.multiple_of(t * cols, cols), cols)
    own_out = []
    for i, (far, near) in enumerate(((h_attn_out, w_attn_out), (h_pool_out, w_pool_out))):
        fetch = pltpu.make_async_copy(far.at[:, mine], near.at[0], local_sem.at[5 + i])
        fetch.start()
        own_out.append(fetch)

    barrier = pltpu.get_barrier_semaphore()
    peers = [(s, flip(t, off)) for off in range(1, m)]
    peers += [(same_parity(i), t) for i in range(1, pairs)]
    peers += [(across, t), (other, t)]
    for peer in peers:
        pl.semaphore_signal(barrier, inc=1, device_id=peer, device_id_type=MESH)
    pl.semaphore_wait(barrier, len(peers))

    def remote(src, dst, send, recv, peer):
        return pltpu.make_async_remote_copy(
            src_ref=src,
            dst_ref=dst,
            send_sem=send,
            recv_sem=recv,
            device_id=peer,
            device_id_type=MESH,
        )

    def push(own, buf, sem, off):
        bit = m // 2
        while bit:
            if off == 0 or bit < (off & -off):
                slot = off ^ bit
                remote(
                    own if off == 0 else buf.at[off],
                    buf.at[slot],
                    sem.at[0, slot],
                    sem.at[1, slot],
                    (s, flip(t, bit)),
                ).start()
            bit //= 2

    def arrive(own, buf, sem, off):
        remote(own, buf.at[off], sem.at[0, off], sem.at[1, off], (s, t)).wait_recv()
        push(own, buf, sem, off)

    def drain(own, buf, sem):
        for slot in range(1, m):
            remote(own, buf.at[slot], sem.at[0, slot], sem.at[1, slot], (s, t)).wait_send()

    push(tokens, tok, tok_sem, 0)

    def share(far, near, sem, off):
        peer = flip(t, off)
        part = pl.ds(pl.multiple_of(peer * cols, cols), cols)
        return remote(far.at[:, part], near.at[off], sem.at[0, off], sem.at[1, off], (s, peer))

    pool_first = [share(h_pool_out, w_pool_out, wp_sem, off) for off in range(1, m)]
    attn_next = [share(h_attn_out, w_attn_out, wa_sem, off) for off in range(1, m)]

    squares = jnp.zeros((rows, 1), f32)

    def ready(off):
        block = flip(t, off)
        raw = (tokens[...] if off == 0 else tok[off]).astype(f32)
        gain = norm_gain[pl.ds(block, 1), :]
        scaled[off] = (raw * gain).astype(bf)
        return jnp.sum(raw * raw, axis=-1, keepdims=True)

    def partial(off, w):
        block = flip(t, off)
        return mm(scaled[off], w[pl.ds(pl.multiple_of(block * cols, cols), cols), :])

    first = list(range(max(m // 2, 1)))
    later = list(range(max(m // 2, 1), m))
    wides = (
        (acc_q, w_query_down),
        (acc_p, w_pool_in),
        (acc_ga, w_gate_attn),
        (acc_gp, w_gate_pool),
    )
    smalls = ((acc_l, w_latent_down), (acc_r, w_rotary))
    for off in first:
        if off:
            arrive(tokens, tok, tok_sem, off)
        squares += ready(off)
        if off == 0:
            for fetch in fetches:
                fetch.wait()
        for acc, w in smalls + wides:
            if off == 0:
                acc[...] = partial(off, w)
            else:
                acc[...] += partial(off, w)
    for off in later:
        arrive(tokens, tok, tok_sem, off)
        if off == later[0]:
            for copy in pool_first + attn_next:
                copy.start()
        squares += ready(off)
        for acc, w in smalls:
            acc[...] += partial(off, w)
    scale = lax.rsqrt(squares / (cols * m) + eps)

    lane = lax.broadcasted_iota(jnp.int32, (rows, LANES), 1)
    low = lane < NOPE

    def rotate(values):
        quarter = ROPE // 2
        partner = jnp.where(
            lane < NOPE + quarter,
            pltpu.roll(values, LANES - quarter, 1),
            pltpu.roll(values, quarter, 1),
        )
        return values * cosine[...] + partner * sine[...]

    def rms(values, gain, width):
        mean = jnp.sum(values * values, axis=-1, keepdims=True) / width
        return values * lax.rsqrt(mean + eps) * gain

    latent = (acc_l[...] * scale).astype(bf).astype(f32)
    latents[0, :, :rank] = rms(latent, latent_gain[...], rank).astype(bf)
    rotary = (acc_r[...] * scale).astype(bf).astype(f32)
    turned = rotate(rotary * gain_k[...])
    latents[0, :, rank:] = jnp.where(low, pltpu.roll(rotary, NOPE, 1), turned).astype(bf)

    core = t % 2
    twin = flip(t, 1)
    my_half = pl.ds(pl.multiple_of(core * half, half), half)
    twin_half = pl.ds(pl.multiple_of((1 - core) * half, half), half)
    near_copy = remote(
        latents.at[0, my_half],
        latents.at[1, my_half],
        near_sem.at[0],
        main_sem.at[1],
        (across, t),
    )
    for i in range(1, pairs):
        slot = 2 * (pairs - i)
        remote(
            latents.at[0, my_half],
            latents.at[slot, my_half],
            near_sem.at[i],
            main_sem.at[slot],
            (same_parity(i), t),
        ).start()
    near_copy.start()

    def main_wait(k):
        remote(
            latents.at[0, my_half],
            latents.at[k, my_half],
            near_sem.at[0],
            main_sem.at[k],
            (s, t),
        ).wait_recv()

    def to_across(k):
        return remote(
            latents.at[k, my_half],
            latents.at[k + 1, my_half],
            far_sem.at[k],
            main_sem.at[k + 1],
            (across, t),
        )

    def to_twin(k):
        return remote(
            latents.at[k, my_half],
            latents.at[k, my_half],
            pair_send.at[k],
            pair_sem.at[k],
            (s, twin),
        )

    def twin_wait(k):
        remote(
            latents.at[k, my_half],
            latents.at[k, twin_half],
            pair_send.at[k],
            pair_sem.at[k],
            (s, twin),
        ).wait_recv()

    def finish(acc, w):
        total = acc[...]
        for off in later:
            total += partial(off, w)
        return total

    pool_input = (finish(acc_p, w_pool_in) * scale).astype(bf).astype(f32)
    padded[pl.ds(REACH, rows), :] = pool_input
    down = remote(
        padded.at[pl.ds(rows, REACH), :],
        padded.at[pl.ds(0, REACH), :],
        halo_sem.at[0],
        halo_sem.at[1],
        ((s + 1) % n, t),
    )
    up = remote(
        padded.at[pl.ds(REACH, REACH), :],
        padded.at[pl.ds(rows + REACH, REACH), :],
        halo_sem.at[2],
        halo_sem.at[3],
        ((s + n - 1) % n, t),
    )
    down.start()
    up.start()

    query_latent = (finish(acc_q, w_query_down) * scale).astype(bf).astype(f32)
    query_normed = rms(query_latent, query_gain[...], query_latent.shape[1]).astype(bf)
    for h in range(heads):
        raw = mm(query_normed, w_query_up[:, h * LANES : (h + 1) * LANES]).astype(bf).astype(f32)
        queries[h] = rotate(rms(raw, gain_q[...], NOPE + ROPE)).astype(bf)
    acc_ga[...] = lax.logistic(finish(acc_ga, w_gate_attn) * scale)
    acc_gp[...] = lax.logistic(finish(acc_gp, w_gate_pool) * scale)

    down.wait_recv()
    up.wait_recv()
    before = padded[pl.ds(0, REACH), :]
    after = padded[pl.ds(rows + REACH, REACH), :]
    padded[pl.ds(0, REACH), :] = before * jnp.where(s > 0, 1.0, 0.0)
    padded[pl.ds(rows + REACH, REACH), :] = after * jnp.where(s < n - 1, 1.0, 0.0)
    groups = w_pool_mix.shape[0]
    position = s * rows + lax.broadcasted_iota(jnp.int32, (rows, 1), 0)
    for j in range(groups):
        group = t * groups + j
        reach = jnp.int32(0)
        for i in range(POOL_GROUPS):
            reach = reach + jnp.where(group == i, 2**i, 0)
        part = slice(j * POOL_GROUP, (j + 1) * POOL_GROUP)
        total = jnp.zeros((rows, POOL_GROUP), f32)
        for shift in range(-REACH, REACH):
            inside = (shift >= -reach) & (shift <= reach - 1)
            total += padded[pl.ds(REACH + shift, rows), part] * jnp.where(inside, 1.0, 0.0)
        start = jnp.maximum(position - reach, 0)
        stop = jnp.minimum(position + reach, rows * n)
        count = (stop - start).astype(f32)
        mixed = (total / count - padded[pl.ds(REACH, rows), part]).astype(bf)
        pool_rows[0, :, part] = (mm(mixed, w_pool_mix[j]) * pool_scale[:, part]).astype(bf)
    push(pool_rows.at[0], pool_rows, pr_sem, 0)

    attn_acc[...] = jnp.zeros_like(attn_acc)
    low_mask = low
    ones = jnp.where(lane == 0, 1.0, 0.0)

    def attend(k):
        latent_block = latents[k, :, :rank]
        turned_block = latents[k, :, rank:].astype(f32)
        shared = jnp.sum(
            jnp.where(low_mask, turned_block * turned_block, 0.0), axis=-1, keepdims=True
        )
        for h in range(heads):
            both = mm(latent_block, w_latent_up[:, h * LANES : (h + 1) * LANES])
            both = both.astype(bf).astype(f32)
            total = jnp.sum(jnp.where(low_mask, both * both, 0.0), axis=-1, keepdims=True)
            level = lax.rsqrt((total + shared) / (NOPE + ROPE) + eps)
            key = (jnp.where(low_mask, both * gain_k[...], turned_block) * level).astype(bf)
            value = jnp.where(low_mask, ones, both).astype(bf)
            scores = lax.dot_general(
                queries[h], key, (((1,), (1,)), ((), ())), preferred_element_type=f32
            )
            attn_acc[h] += mm(jnp.exp2(scores).astype(bf), value)

    def step(i, carry):
        @pl.when(i + 1 < pairs)
        def _():
            main_wait(2 * i + 2)
            to_across(2 * i + 2).start()
            to_twin(2 * i + 2).start()

        @pl.when(i > 0)
        def _():
            twin_wait(2 * i)

        attend(2 * i)
        main_wait(2 * i + 1)
        to_twin(2 * i + 1).start()
        twin_wait(2 * i + 1)
        attend(2 * i + 1)
        return carry

    lax.fori_loop(0, pairs, step, 0)

    for j in range(heads // 2):
        even = attn_acc[2 * j]
        odd = attn_acc[2 * j + 1]
        even = even / even[:, :1]
        odd = odd / odd[:, :1]
        attn_rows[0, :, j * LANES : (j + 1) * LANES] = jnp.where(
            low, pltpu.roll(even, NOPE, 1), odd
        ).astype(bf)
    push(attn_rows.at[0], attn_rows, ar_sem, 0)

    for off in range(1, m):
        arrive(pool_rows.at[0], pool_rows, pr_sem, off)
    for fetch in own_out:
        fetch.wait()
    for copy in pool_first + attn_next:
        copy.wait_recv()
    pool_branch = mm(pool_rows[0], w_pool_out[0])
    for off in range(1, m):
        pool_branch += mm(pool_rows[off], w_pool_out[off])
    acc_gp[...] *= pool_branch
    attn_branch = mm(attn_rows[0], w_attn_out[0])
    for off in range(1, m):
        arrive(attn_rows.at[0], attn_rows, ar_sem, off)
        attn_branch += mm(attn_rows[off], w_attn_out[off])
    out[...] = (acc_ga[...] * attn_branch + acc_gp[...]).astype(bf)

    drain(tokens, tok, tok_sem)
    drain(pool_rows.at[0], pool_rows, pr_sem)
    drain(attn_rows.at[0], attn_rows, ar_sem)
    for copy in pool_first + attn_next:
        copy.wait_send()
    down.wait_send()
    up.wait_send()
    for i in range(pairs):
        remote(
            latents.at[0, my_half], latents.at[0, my_half], near_sem.at[i], main_sem.at[1], (s, t)
        ).wait_send()
    for k in range(1, n):
        to_twin(k).wait_send()
        if k % 2 == 0:
            to_across(k).wait_send()


def body(
    n,
    m,
    tokens,
    norm_gain,
    w_query_down,
    query_gain,
    w_query_up,
    w_latent_down,
    latent_gain,
    w_rotary_key,
    w_latent_up,
    query_head_gain,
    key_head_gain,
    w_pool_in,
    w_pool_mix,
    pool_scale,
    w_attn_out,
    w_pool_out,
    w_gate_attn,
    w_gate_pool,
):
    rows, cols = tokens.shape
    width = NOPE + ROPE
    heads = w_query_up.shape[1] // width
    rank = w_latent_down.shape[1]
    pool = w_pool_in.shape[1]
    spare = LANES - width
    positions = lax.axis_index("sp") * rows + jnp.arange(rows, dtype=jnp.int32)
    freqs = theta ** (-jnp.arange(ROPE // 2, dtype=f32) / (ROPE // 2))
    angles = positions.astype(f32)[:, None] * freqs[None, :]
    cos = jnp.cos(angles)
    sin = jnp.sin(angles)
    cosine = jnp.concatenate(
        [jnp.ones((rows, NOPE), f32), cos, cos, jnp.zeros((rows, spare), f32)], axis=1
    )
    sine = jnp.concatenate(
        [jnp.zeros((rows, NOPE), f32), -sin, sin, jnp.zeros((rows, spare), f32)], axis=1
    )
    query_up = jnp.pad(
        w_query_up.reshape(-1, heads, width), ((0, 0), (0, 0), (0, spare))
    ).reshape(-1, heads * LANES)
    rotary = jnp.pad(w_rotary_key, ((0, 0), (NOPE, spare)))
    gain_q = jnp.pad(query_head_gain * (width**-0.5 * math.log2(math.e)), (0, spare))[None, :]
    gain_k = jnp.pad(key_head_gain, (0, spare))[None, :]
    dma = pltpu.SemaphoreType.DMA
    near = pl.BlockSpec(memory_space=pltpu.VMEM)
    far = pl.BlockSpec(memory_space=pl.ANY)
    return pl.pallas_call(
        functools.partial(kernel, n, m),
        out_shape=jax.ShapeDtypeStruct((rows, cols), bf),
        in_specs=[near] * 13 + [far] * 7,
        out_specs=near,
        scratch_shapes=[
            pltpu.VMEM(w_query_down.shape, bf),
            pltpu.VMEM(w_latent_down.shape, bf),
            pltpu.VMEM(w_pool_in.shape, bf),
            pltpu.VMEM(w_gate_attn.shape, bf),
            pltpu.VMEM(w_gate_pool.shape, bf),
            pltpu.VMEM((m, w_attn_out.shape[0], cols), bf),
            pltpu.VMEM((m, w_pool_out.shape[0], cols), bf),
            pltpu.VMEM((m, rows, cols), bf),
            pltpu.VMEM((m, rows, cols), bf),
            pltpu.VMEM((rows, w_query_down.shape[1]), f32),
            pltpu.VMEM((rows, rank), f32),
            pltpu.VMEM((rows, LANES), f32),
            pltpu.VMEM((rows, pool), f32),
            pltpu.VMEM((rows, cols), f32),
            pltpu.VMEM((rows, cols), f32),
            pltpu.VMEM((heads, rows, LANES), bf),
            pltpu.VMEM((n, rows, rank + LANES), bf),
            pltpu.VMEM((heads, rows, LANES), f32),
            pltpu.VMEM((rows + 2 * REACH, pool), f32),
            pltpu.VMEM((m, rows, heads * VALUE_DIM), bf),
            pltpu.VMEM((m, rows, pool), bf),
            dma((7,)),
            dma((2, m)),
            dma((2, m)),
            dma((2, m)),
            dma((2, m)),
            dma((2, m)),
            dma((4,)),
            dma((n // 2,)),
            dma((n,)),
            dma((n,)),
            dma((n,)),
            dma((n,)),
        ],
        compiler_params=pltpu.CompilerParams(collective_id=0, has_side_effects=True),
    )(
        tokens,
        norm_gain.reshape(m, cols),
        query_gain[None, :],
        query_up,
        latent_gain[None, :],
        rotary,
        w_latent_up,
        gain_q,
        gain_k,
        w_pool_mix,
        pool_scale[None, :],
        cosine,
        sine,
        w_query_down,
        w_latent_down,
        w_pool_in,
        w_gate_attn,
        w_gate_pool,
        w_attn_out,
        w_pool_out,
    )


def solution(mesh):
    placed = (
        P("sp", "tp"),
        P(),
        P(),
        P(),
        P(None, "tp"),
        P(),
        P(),
        P(),
        P(None, "tp"),
        P(),
        P(),
        P(None, "tp"),
        P("tp", None, None),
        P("tp"),
        P("tp", None),
        P("tp", None),
        P(None, "tp"),
        P(None, "tp"),
    )
    held = functools.partial(body, mesh.shape["sp"], mesh.shape["tp"])
    return jax.shard_map(held, mesh=mesh, in_specs=placed, out_specs=P("sp", "tp"), check_vma=False)
```

time: 214 us -> 74.6 us (0.35)
  Pallas kernels: 0 us -> 64.6 us
  matrix products: 50.5 us -> 0 us
  waiting for transfers between devices: 36.9 us -> 0 us
  starting transfers between devices: 29.3 us -> 0 us
  blocking collectives: 25.2 us -> 0 us
  other arithmetic: 26.5 us -> 2.44 us
  local copies, waits for them, and re-layouts: 23.5 us -> 7.22 us
  between operations: 13.7 us -> 0.09 us
  loops' own time: 6.1 us -> 0 us
    pallas_call x0 -> x1, Pallas kernels: none -> 64.6 us  [body(): pl.pallas_call(functools.partial(kernel, n, m), out_shape=jax.ShapeDtypeS...]
    dot_general x34 -> x0, matrix products: 50.5 us -> none  [the longest x8 16 us: one_block(): jnp.einsum('qhd,khd->hqk', query, key, preferred_element_type=jnp.float32)]
    all_gather x1 -> x0, blocking collectives: 25.2 us -> none  [body(): rotary_piece = lax.all_gather(rotary_key, 'sp', axis=0, tiled=True)]
    all_to_all x4 -> x0, starting transfers between devices: 23.9 us -> none  [the longest x1 11.5 us: body(): lax.all_to_all(pool_rows, 'tp', split_axis=0, concat_axis=1, tiled=True)]
    all_gather x4 -> x0, waiting for transfers between devices: 23.7 us -> none  [the longest x1 23.7 us: body(): whole = lax.all_gather(tokens, 'tp', axis=1, tiled=True)]
    reduce_sum x18 -> x0, other arithmetic: 19.9 us -> none  [the longest x8 17.4 us: one_block(): total = total * factor + jnp.sum(expo, axis=-1)]
    all_to_all x4 -> x0, waiting for transfers between devices: 11.3 us -> none  [the longest x1 5.47 us: body(): lax.all_to_all(pool_here.astype(jnp.bfloat16), 'tp', split_axis=1, concat...]
    another operation x1 -> x0, loops' own time: 6.1 us -> none  [body(): lax.scan(one_block, start_state, (latent_blocks, rotary_blocks, jnp.arang...]
  transfers between devices with their start and end apart: 10 -> 0, of which waited for: 4 -> 0; matrix products, arithmetic and copies ran while one was open for 41% -> 0% of each run, Pallas kernels for 0% -> 0%
where the time goes in v1:
time: 74.6 us; the launch traced here: 74.4 us
  Pallas kernels  64.6 us (87%)
  local copies, waits for them, and re-layouts  7.22 us (10%)
  other arithmetic  2.44 us (3%)
    pallas_call x1, Pallas kernels, body(): pl.pallas_call(functools.partial(kernel, n, m), out_shape=jax.ShapeDtypeS...  64.6 us
    unnamed x7, local copies, waits for them, and re-layouts  3.23 us

profile of v1, /device:TPU:1, one launch (start us, length us, event | category | flops | bytes accessed | tf_op | source)
XLA Modules:
  0.0 74.4 jit_solution(14011034834218065143)
XLA Ops:
  0.0 0.0 copy-start
  0.0 0.8 %fusion = (f32[384,16]{1,0:T(8,128)S(1)}, f32[384,16]{1,0:T(8,128)S(1)}, f32[384,16]{1,0:T(8,128)S(1)}) fusion(f32[16]{0:T(128)S(1)} %multiply_power_fusion, f32[384]{0:T(512)S(1)} %add_convert_fusion), kind=kLoop, calls=%fused_computation.4 | loop fusion | flops 12288 | bytes 75328 | tf_op jit(solution)/shard_map/neg | solution.py:486
  0.9 0.1 pad.26.clone
  0.9 1.0 %maximum_maximum_fusion.1 = (f32[384,128]{1,0:T(8,128)}, f32[384,128]{1,0:T(8,128)}) fusion(f32[384,16]{1,0:T(8,128)S(1)} %get-tuple-element.6, f32[384,16]{1,0:T(8,128)S(1)} %get-tuple-element.5, f32[128]{0:T(128)S(1)} %pad.19.clone, f32[128]{0:T(128)S(1)} %pad.26.clone, f32[384,16]{1,0:T(8,128)S(1)} %get-tuple-element.7, f32[128]{0:T(128)S(1)} %pad.23.clone), kind=kLoop, calls=%fused_computation.3 | loop fusion | flops 294912 | bytes 468480 | tf_op jit(solution)/shard_map/concatenate | solution.py:485
  1.9 0.7 broadcast_multiply_fusion
  2.6 1.2 %pad_bitcast_fusion = (f32[1,128]{1,0:T(1,128)}, f32[1,128]{1,0:T(1,128)}) fusion(f32[96]{0:T(128)} %param.28, f32[96]{0:T(128)S(1)} %broadcast_multiply_fusion), kind=kLoop, calls=%fused_computation.7 | loop fusion | bytes 1792 | tf_op jit(solution)/shard_map/broadcast_in_dim | solution.py:493
  3.8 0.0 copy-start.1
  3.8 1.2 %copy.23 = bf16[512,384]{0,1:T(8,128)(2,1)S(1)} copy(bf16[512,384]{1,0:T(8,128)(2,1)} %param.22) | data formatting | bytes 786432 | tf_op args[4]
  5.1 1.0 %copy.27.w_query_up = bf16[512,512]{1,0:T(8,128)(2,1)} copy(bf16[512,512]{0,1:T(8,128)(2,1)S(1)} %bitcast.9) | data formatting | bytes 1048576 | tf_op jit(solution)/shard_map/reshape | solution.py:490
  6.1 0.0 copy-done
  6.1 0.3 copy.25
  6.3 1.0 %pad.16.w_rotary = bf16[2048,128]{1,0:T(8,128)(2,1)} pad(bf16[2048,32]{1,0:T(8,128)(2,1)S(1)} %copy.25, bf16[]{:T(256)} %constant.9.clone.1), padding=0_0x64_32 | pad | bytes 655362 | tf_op jit(solution)/shard_map/jit(_pad)/pad | solution.py:491
  7.4 0.0 copy-done.1
  7.4 0.6 reshape.20.norm_gain
  8.0 64.6 %shard_map.172 = bf16[384,512]{1,0:T(8,128)(2,1)} custom-call(bf16[384,512]{1,0:T(8,128)(2,1)} %tokens.1, f32[4,512]{1,0:T(4,128)} %reshape.20.norm_gain, f32[1,512]{1,0:T(1,128)} %bitcast.11, bf16[512,512]{1,0:T(8,128)(2,1)} %copy.27.w_query_up, f32[1,256]{1,0:T(1,128)} %bitcast.12, bf16[2048,128]{1,0:T(8,128)(2,1)} %pad.16.w_rotary, ...), custom_call_target="tpu_custom_call" | custom-call | tf_op jit(solution)/shard_map/pallas_call | solution.py:497
  72.6 1.8 %copy.29 = bf16[384,512]{1,0:T(8,128)(2,1)} copy(bf16[384,512]{1,0:T(8,128)(2,1)} %shard_map.172) | data formatting | bytes 786432
  (8 shorter events, 0.1 us)
Async XLA Ops:
  0.0 6.1 %copy-start = (bf16[2048,32]{0,1:T(8,128)(2,1)S(1)}, bf16[2048,32]{0,1:T(8,128)(2,1)}, u32[]{:S(2)}) copy-start(bf16[2048,32]{0,1:T(8,128)(2,1)} %param.25) | copy-start | bytes 393220
  3.8 3.5 %copy-start.1 = (f32[2048]{0:T(1024)S(1)}, f32[2048]{0:T(1024)}, u32[]{:S(2)}) copy-start(f32[2048]{0:T(1024)} %param.19) | copy-start | bytes 24580

commit v2 on v1

--- a/solution.py
+++ b/solution.py
@@ -2,6 +2,7 @@
 import math
 
 import jax
+import numpy as np
 import jax.numpy as jnp
 from jax import lax
 from jax.experimental import pallas as pl
@@ -44,14 +45,13 @@
     query_gain,
     w_query_up,
     latent_gain,
-    w_rotary,
     w_latent_up,
     gain_q,
     gain_k,
     w_pool_mix,
     pool_scale,
-    cosine,
-    sine,
+    freqs,
+    h_rotary,
     h_query_down,
     h_latent_down,
     h_pool_in,
@@ -60,6 +60,9 @@
     h_attn_out,
     h_pool_out,
     out,
+    cosine,
+    sine,
+    w_rotary,
     w_query_down,
     w_latent_down,
     w_pool_in,
@@ -106,6 +109,10 @@
     heads = attn_acc.shape[0]
     rank = latents.shape[2] - LANES
 
+    def gap_of(i):
+        odd = i % 2
+        return odd * ((i + 1) // 2) + (1 - odd) * ((pairs - i // 2) % pairs)
+
     def same_parity(i):
         return ((p + i) % pairs) * 2 + y
 
@@ -117,6 +124,7 @@
             (h_pool_in, w_pool_in),
             (h_gate_attn, w_gate_attn),
             (h_gate_pool, w_gate_pool),
+            (h_rotary, w_rotary),
         )
     ):
         fetch = pltpu.make_async_copy(far, near, local_sem.at[i])
@@ -125,7 +133,7 @@
     mine = pl.ds(pl.multiple_of(t * cols, cols), cols)
     own_out = []
     for i, (far, near) in enumerate(((h_attn_out, w_attn_out), (h_pool_out, w_pool_out))):
-        fetch = pltpu.make_async_copy(far.at[:, mine], near.at[0], local_sem.at[5 + i])
+        fetch = pltpu.make_async_copy(far.at[:, mine], near.at[0], local_sem.at[6 + i])
         fetch.start()
         own_out.append(fetch)
 
@@ -180,11 +188,22 @@
     attn_next = [share(h_attn_out, w_attn_out, wa_sem, off) for off in range(1, m)]
 
     squares = jnp.zeros((rows, 1), f32)
+    lane = lax.broadcasted_iota(jnp.int32, (rows, LANES), 1)
+    low = lane < NOPE
+    spare = LANES - NOPE - ROPE
+    place = s * rows + lax.broadcasted_iota(jnp.int32, (rows, LANES), 0)
+    angles = place.astype(f32) * freqs[...]
+    cosine[...] = jnp.cos(angles)
+    sine[...] = jnp.sin(angles) * jnp.where(lane < NOPE + ROPE // 2, -1.0, 1.0)
+    nothing = jnp.zeros((1, spare), f32)
+    gain_q = jnp.concatenate([gain_q[...], nothing], axis=1)
+    gain_q = gain_q * ((NOPE + ROPE) ** -0.5 * math.log2(math.e))
+    gain_k = jnp.concatenate([gain_k[...], nothing], axis=1)
 
     def ready(off):
         block = flip(t, off)
         raw = (tokens[...] if off == 0 else tok[off]).astype(f32)
-        gain = norm_gain[pl.ds(block, 1), :]
+        gain = norm_gain[:, pl.ds(pl.multiple_of(block * cols, cols), cols)]
         scaled[off] = (raw * gain).astype(bf)
         return jnp.sum(raw * raw, axis=-1, keepdims=True)
 
@@ -223,9 +242,6 @@
             acc[...] += partial(off, w)
     scale = lax.rsqrt(squares / (cols * m) + eps)
 
-    lane = lax.broadcasted_iota(jnp.int32, (rows, LANES), 1)
-    low = lane < NOPE
-
     def rotate(values):
         quarter = ROPE // 2
         partner = jnp.where(
@@ -242,7 +258,10 @@
     latent = (acc_l[...] * scale).astype(bf).astype(f32)
     latents[0, :, :rank] = rms(latent, latent_gain[...], rank).astype(bf)
     rotary = (acc_r[...] * scale).astype(bf).astype(f32)
-    turned = rotate(rotary * gain_k[...])
+    rotary = jnp.concatenate(
+        [jnp.zeros((rows, NOPE), f32), rotary, jnp.zeros((rows, spare), f32)], axis=1
+    )
+    turned = rotate(rotary * gain_k)
     latents[0, :, rank:] = jnp.where(low, pltpu.roll(rotary, NOPE, 1), turned).astype(bf)
 
     core = t % 2
@@ -257,13 +276,14 @@
         (across, t),
     )
     for i in range(1, pairs):
-        slot = 2 * (pairs - i)
+        gap = gap_of(i)
+        slot = 2 * gap
         remote(
             latents.at[0, my_half],
             latents.at[slot, my_half],
             near_sem.at[i],
             main_sem.at[slot],
-            (same_parity(i), t),
+            (same_parity(pairs - gap), t),
         ).start()
     near_copy.start()
 
@@ -330,9 +350,11 @@
 
     query_latent = (finish(acc_q, w_query_down) * scale).astype(bf).astype(f32)
     query_normed = rms(query_latent, query_gain[...], query_latent.shape[1]).astype(bf)
+    query_raw = mm(query_normed, w_query_up[...]).astype(bf).astype(f32)
     for h in range(heads):
-        raw = mm(query_normed, w_query_up[:, h * LANES : (h + 1) * LANES]).astype(bf).astype(f32)
-        queries[h] = rotate(rms(raw, gain_q[...], NOPE + ROPE)).astype(bf)
+        raw = query_raw[:, h * (NOPE + ROPE) : (h + 1) * (NOPE + ROPE)]
+        raw = jnp.concatenate([raw, jnp.zeros((rows, spare), f32)], axis=1)
+        queries[h] = rotate(rms(raw, gain_q, NOPE + ROPE)).astype(bf)
     acc_ga[...] = lax.logistic(finish(acc_ga, w_gate_attn) * scale)
     acc_gp[...] = lax.logistic(finish(acc_gp, w_gate_pool) * scale)
 
@@ -376,7 +398,7 @@
             both = both.astype(bf).astype(f32)
             total = jnp.sum(jnp.where(low_mask, both * both, 0.0), axis=-1, keepdims=True)
             level = lax.rsqrt((total + shared) / (NOPE + ROPE) + eps)
-            key = (jnp.where(low_mask, both * gain_k[...], turned_block) * level).astype(bf)
+            key = (jnp.where(low_mask, both * gain_k, turned_block) * level).astype(bf)
             value = jnp.where(low_mask, ones, both).astype(bf)
             scores = lax.dot_general(
                 queries[h], key, (((1,), (1,)), ((), ())), preferred_element_type=f32
@@ -384,21 +406,24 @@
             attn_acc[h] += mm(jnp.exp2(scores).astype(bf), value)
 
     def step(i, carry):
+        now = 2 * gap_of(i)
+
         @pl.when(i + 1 < pairs)
         def _():
-            main_wait(2 * i + 2)
-            to_across(2 * i + 2).start()
-            to_twin(2 * i + 2).start()
+            ahead = 2 * gap_of(i + 1)
+            main_wait(ahead)
+            to_across(ahead).start()
+            to_twin(ahead).start()
 
         @pl.when(i > 0)
         def _():
-            twin_wait(2 * i)
-
-        attend(2 * i)
-        main_wait(2 * i + 1)
-        to_twin(2 * i + 1).start()
-        twin_wait(2 * i + 1)
-        attend(2 * i + 1)
+            twin_wait(now)
+
+        attend(now)
+        main_wait(now + 1)
+        to_twin(now + 1).start()
+        twin_wait(now + 1)
+        attend(now + 1)
         return carry
 
     lax.fori_loop(0, pairs, step, 0)
@@ -473,33 +498,21 @@
     heads = w_query_up.shape[1] // width
     rank = w_latent_down.shape[1]
     pool = w_pool_in.shape[1]
-    spare = LANES - width
-    positions = lax.axis_index("sp") * rows + jnp.arange(rows, dtype=jnp.int32)
-    freqs = theta ** (-jnp.arange(ROPE // 2, dtype=f32) / (ROPE // 2))
-    angles = positions.astype(f32)[:, None] * freqs[None, :]
-    cos = jnp.cos(angles)
-    sin = jnp.sin(angles)
-    cosine = jnp.concatenate(
-        [jnp.ones((rows, NOPE), f32), cos, cos, jnp.zeros((rows, spare), f32)], axis=1
-    )
-    sine = jnp.concatenate(
-        [jnp.zeros((rows, NOPE), f32), -sin, sin, jnp.zeros((rows, spare), f32)], axis=1
-    )
-    query_up = jnp.pad(
-        w_query_up.reshape(-1, heads, width), ((0, 0), (0, 0), (0, spare))
-    ).reshape(-1, heads * LANES)
-    rotary = jnp.pad(w_rotary_key, ((0, 0), (NOPE, spare)))
-    gain_q = jnp.pad(query_head_gain * (width**-0.5 * math.log2(math.e)), (0, spare))[None, :]
-    gain_k = jnp.pad(key_head_gain, (0, spare))[None, :]
+    freqs = theta ** (-(np.arange(LANES) % (ROPE // 2)) / (ROPE // 2))
+    freqs = np.where(np.arange(LANES) // ROPE == NOPE // ROPE, freqs, 0.0)
+    freqs = jnp.asarray(freqs, f32)[None, :]
     dma = pltpu.SemaphoreType.DMA
     near = pl.BlockSpec(memory_space=pltpu.VMEM)
     far = pl.BlockSpec(memory_space=pl.ANY)
     return pl.pallas_call(
         functools.partial(kernel, n, m),
         out_shape=jax.ShapeDtypeStruct((rows, cols), bf),
-        in_specs=[near] * 13 + [far] * 7,
+        in_specs=[near] * 11 + [far] * 8,
         out_specs=near,
         scratch_shapes=[
+            pltpu.VMEM((rows, LANES), f32),
+            pltpu.VMEM((rows, LANES), f32),
+            pltpu.VMEM(w_rotary_key.shape, bf),
             pltpu.VMEM(w_query_down.shape, bf),
             pltpu.VMEM(w_latent_down.shape, bf),
             pltpu.VMEM(w_pool_in.shape, bf),
@@ -511,7 +524,7 @@
             pltpu.VMEM((m, rows, cols), bf),
             pltpu.VMEM((rows, w_query_down.shape[1]), f32),
             pltpu.VMEM((rows, rank), f32),
-            pltpu.VMEM((rows, LANES), f32),
+            pltpu.VMEM((rows, ROPE), f32),
             pltpu.VMEM((rows, pool), f32),
             pltpu.VMEM((rows, cols), f32),
             pltpu.VMEM((rows, cols), f32),
@@ -521,7 +534,7 @@
             pltpu.VMEM((rows + 2 * REACH, pool), f32),
             pltpu.VMEM((m, rows, heads * VALUE_DIM), bf),
             pltpu.VMEM((m, rows, pool), bf),
-            dma((7,)),
+            dma((8,)),
             dma((2, m)),
             dma((2, m)),
             dma((2, m)),
@@ -537,18 +550,17 @@
         compiler_params=pltpu.CompilerParams(collective_id=0, has_side_effects=True),
     )(
         tokens,
-        norm_gain.reshape(m, cols),
+        norm_gain[None, :],
         query_gain[None, :],
-        query_up,
+        w_query_up,
         latent_gain[None, :],
-        rotary,
         w_latent_up,
-        gain_q,
-        gain_k,
+        query_head_gain[None, :],
+        key_head_gain[None, :],
         w_pool_mix,
         pool_scale[None, :],
-        cosine,
-        sine,
+        freqs,
+        w_rotary_key,
         w_query_down,
         w_latent_down,
         w_pool_in,

time: 74.6 us -> 68.1 us (0.913)
  local copies, waits for them, and re-layouts: 7.22 us -> 3.67 us
  other arithmetic: 2.44 us -> 0 us
    reshape x2 -> x0, local copies, waits for them, and re-layouts: 1.61 us -> none  [the longest x1 1.01 us: body(): query_up = jnp.pad(w_query_up.reshape(-1, heads, width), ((0, 0), (0, 0),...]
    broadcast_in_dim x3 -> x0, local copies, waits for them, and re-layouts: 1.24 us -> none  [the longest x1 1.23 us: body(): gain_k = jnp.pad(key_head_gain, (0, spare))[None, :]]
    pad x2 -> x0, local copies, waits for them, and re-layouts: 1.06 us -> none  [the longest x1 1.02 us: body(): rotary = jnp.pad(w_rotary_key, ((0, 0), (NOPE, spare)))]
    concatenate x1 -> x0, other arithmetic: 1.01 us -> none  [body(): jnp.concatenate([jnp.zeros((rows, NOPE), f32), -sin, sin, jnp.zeros((rows...]
    neg x1 -> x0, other arithmetic: 0.76 us -> none  [body(): -sin]
    unnamed x7 -> x2, local copies, waits for them, and re-layouts: 3.23 us -> 3.67 us
where the time goes in v2:
time: 68.1 us; the launch traced here: 67.9 us
  Pallas kernels  64.2 us (94%)
  local copies, waits for them, and re-layouts  3.67 us (5%)
    pallas_call x1, Pallas kernels, body(): pl.pallas_call(functools.partial(kernel, n, m), out_shape=jax.ShapeDtypeS...  64.2 us
    unnamed x2, local copies, waits for them, and re-layouts  3.67 us

profile of v2, /device:TPU:1, one launch (start us, length us, event | category | flops | bytes accessed | tf_op | source)
XLA Modules:
  0.0 67.9 jit_solution(5902671332173431730)
XLA Ops:
  0.0 1.9 %copy.20.h_rotary = bf16[2048,32]{1,0:T(8,128)(2,1)} copy(bf16[2048,32]{0,1:T(8,128)(2,1)} %param.26) | data formatting | bytes 262144 | tf_op args[7]
  1.9 64.2 %shard_map.181 = bf16[384,512]{1,0:T(8,128)(2,1)} custom-call(bf16[384,512]{1,0:T(8,128)(2,1)} %tokens.1, f32[1,2048]{1,0:T(1,128)} %bitcast.6, f32[1,512]{1,0:T(1,128)} %bitcast.7, bf16[512,384]{1,0:T(8,128)(2,1)} %w_query_up.1, f32[1,256]{1,0:T(1,128)} %bitcast.8, bf16[256,512]{1,0:T(8,128)(2,1)} %w_latent_up.1, f32[1,96]{1,0:T(1,128)} %bitcast.10, ...), custom_call_target="tpu_custom_call" | custom-call | tf_op jit(solution)/shard_map/pallas_call | solution.py:507
  66.1 1.8 %copy.22 = bf16[384,512]{1,0:T(8,128)(2,1)} copy(bf16[384,512]{1,0:T(8,128)(2,1)} %shard_map.181) | data formatting | bytes 786432
